TPU v7x, 32 devices: a whole 2x2x4 slice. The times are simulated.
32 devices in a mesh: ep: 4 (over z), tp: 8 (over y, x, core).
Axes of the slice: x: 2, y: 2, z: 4, core: 2. Of those that a mesh axis runs over, the one named last changes fastest.
Arguments:
- tokens: bfloat16 [4096, 2048], P(('ep', 'tp')), may hold values from -40 to 40
- norm_gain: float32 [2048], replicated, may hold values from 0.1 to 1.9
- routes: int32 [4096, 2], P(('ep', 'tp')), may hold values from 0 to 7, all different within a row; in each aligned block of 128 rows (0 to 127, 128 to 255, ...) at most 64 rows name the same one
- gates: float32 [4096, 2], P(('ep', 'tp')), may hold values from 0.25 to 2
- expert_gate: bfloat16 [8, 2048, 512], P('tp'), may hold values from -0.125 to 0.125
- expert_up: bfloat16 [8, 2048, 512], P('tp'), may hold values from -0.125 to 0.125
- expert_down: bfloat16 [8, 512, 2048], P('tp'), may hold values from -0.25 to 0.25
- shared_gate: bfloat16 [2048, 256], replicated, may hold values from -0.125 to 0.125
- shared_up: bfloat16 [2048, 256], replicated, may hold values from -0.125 to 0.125
- shared_down: bfloat16 [256, 2048], replicated, may hold values from -0.375 to 0.375
Outputs:
- mixed: bfloat16 [4096, 2048], P(('ep', 'tp'))
- load: float32 [8], replicated
Inputs may be any that keep to these rules, and one draw needn't show every extreme that they name: `routes`: each row names 2 different experts. Among the rows of one device no expert is named by more than 64 rows, and in every draw some expert is named by exactly 64 rows of some device.
All inputs are finite; a program needn't handle non-finite values.
Results may differ from a plain program's by a relative error of at most 0.002.
The roundings to bfloat16 on the way count: a program that leaves them out, or rounds other values in their place, can miss the bound.
Values may be sent and summed in bfloat16 or wider, within the bound.
A program may use at most 64 MiB of HBM per device.

v0:
```python
import functools

import jax
import jax.numpy as jnp
from jax import lax
from jax.experimental import pallas as pl
from jax.experimental.pallas import tpu as pltpu
from jax.sharding import PartitionSpec as P

F32 = jnp.float32
BF16 = jnp.bfloat16


def kernel(
    n,
    eps,
    cap,
    tokens_hbm,
    routes,
    gates,
    gain,
    expert_gate,
    expert_up,
    expert_down,
    shared_gate,
    shared_up,
    shared_down,
    out,
    load,
    tokens,
    blocks,
    group_routes,
    every_routes,
    rows_in,
    hidden,
    results,
    returned,
    total,
    w_gate,
    w_up,
    w_down,
    s_gate,
    s_up,
    s_down,
    weight_sem,
    own_sem,
    route_send,
    route_recv,
    far_send,
    far_recv,
    token_send,
    token_recv,
    result_send,
    result_recv,
):
    me = lax.axis_index("tp")
    here = lax.axis_index("ep")
    rows, width = tokens.shape
    half = rows // 2
    chunk = rows // cap
    relay = n == 8
    order = [lax.rem(me + i, n) for i in range(n)]
    if relay:
        core, xbit, ybit = me % 2, (me // 2) % 2, me // 4
        across = 1 - 2 * core
        sib = me + across
        nx = me + 2 * (1 - 2 * xbit)
        ny = me + 4 * (1 - 2 * ybit)
        nd = nx + 4 * (1 - 2 * ybit)
        order = [me, sib, nx, nx + across, ny, ny + across, nd, nd + across]

    barrier = pltpu.get_barrier_semaphore()
    planes = [lax.rem(here + i, eps) for i in range(1, eps)]
    for peer in order[1:]:
        pl.semaphore_signal(barrier, inc=1, device_id={"tp": peer})
    for plane in planes:
        pl.semaphore_signal(barrier, inc=1, device_id={"ep": plane})
    own_tokens = pltpu.make_async_copy(tokens_hbm, tokens, own_sem.at[1])
    own_tokens.start()

    weights = [
        pltpu.make_async_copy(src, dst, weight_sem.at[i])
        for i, (src, dst) in enumerate(
            [
                (expert_gate.at[0], w_gate),
                (expert_up.at[0], w_up),
                (expert_down.at[0], w_down),
                (shared_gate, s_gate),
                (shared_up, s_up),
                (shared_down, s_down),
            ]
        )
    ]
    for copy in weights:
        copy.start()
    own_routes = pltpu.make_async_copy(routes, group_routes.at[me], own_sem.at[0])
    own_routes.start()

    pl.semaphore_wait(barrier, n - 1 + eps - 1)

    pending = []
    for i, peer in enumerate(order[1:]):
        copy = pltpu.make_async_remote_copy(
            src_ref=routes,
            dst_ref=group_routes.at[me],
            send_sem=route_send.at[i],
            recv_sem=route_recv.at[me],
            device_id={"tp": peer},
        )
        copy.start()
        pending.append(copy)

    def part(ref, piece):
        return ref.at[pl.ds(piece * half, half)]

    def send(source, piece, slot, peer, number):
        copy = pltpu.make_async_remote_copy(
            src_ref=part(source, piece),
            dst_ref=part(blocks.at[slot], piece),
            send_sem=token_send.at[number],
            recv_sem=token_recv.at[slot, piece],
            device_id={"tp": peer},
        )
        copy.start()
        pending.append(copy)

    def landed(slot, piece):
        ref = part(blocks.at[slot], piece)
        pltpu.make_async_copy(ref, ref, token_recv.at[slot, piece]).wait()

    own_tokens.wait()
    if relay:
        send(tokens, 0, me, nx, 0)
        send(tokens, 1, me, ny, 1)
        send(tokens, 1, me, nx, 2)
        send(tokens, 0, me, ny, 3)
        send(tokens, 0, me, sib, 4)
        send(tokens, 1, me, sib, 5)
    else:
        for i, peer in enumerate(order[1:]):
            send(tokens, 0, me, peer, 2 * i)
            send(tokens, 1, me, peer, 2 * i + 1)

    earlier = (
        lax.broadcasted_iota(jnp.int32, (rows, rows), 0)
        < lax.broadcasted_iota(jnp.int32, (rows, rows), 1)
    ).astype(BF16)
    row_in_slot = lax.broadcasted_iota(jnp.int32, (cap, rows), 0)

    def normed_of(values):
        center = jnp.mean(values, axis=-1, keepdims=True)
        values = values - center
        spread = jnp.mean(jnp.square(values), axis=-1, keepdims=True)
        return (values * lax.rsqrt(spread + 1e-05) * gain[...]).astype(BF16)

    def gated(values, gate_ref, up_ref):
        gate_part = jnp.dot(values, gate_ref[...], preferred_element_type=F32)
        up_part = jnp.dot(values, up_ref[...], preferred_element_type=F32)
        return (gate_part * (1.0 / (1.0 + jnp.exp(-gate_part))) * up_part).astype(BF16)

    def gather(i, at):
        source = order[i]
        named = group_routes[source]
        member = (named[0:1] == me) | (named[1:2] == me)
        count = jnp.dot(
            jnp.broadcast_to(member.astype(F32), (8, rows)).astype(BF16),
            earlier,
            preferred_element_type=F32,
        )[0:1].astype(jnp.int32)
        slot = jnp.where(member, count, -1)
        pick = (row_in_slot == slot).astype(F32).astype(BF16)
        held = tokens[...] if i == 0 else blocks[source]
        taken = jnp.dot(pick, held, preferred_element_type=F32)
        rows_in[at * cap : (at + 1) * cap, :] = normed_of(taken)

    tile = 512

    def expert(members):
        count = len(members) * cap
        hidden[:count] = gated(rows_in[:count], w_gate, w_up)
        for at in range(0, width, tile):
            value = jnp.dot(
                hidden[:count], w_down[:, at : at + tile], preferred_element_type=F32
            ).astype(BF16)
            for g, i in enumerate(members):
                piece = value[g * cap : (g + 1) * cap]
                if i == 0:
                    returned[me, :, at : at + tile] = piece
                else:
                    results[i, :, at : at + tile] = piece
        for i in members:
            if i == 0:
                continue
            copy = pltpu.make_async_remote_copy(
                src_ref=results.at[i],
                dst_ref=returned.at[me],
                send_sem=result_send.at[i],
                recv_sem=result_recv.at[me],
                device_id={"tp": order[i]},
            )
            copy.start()
            pending.append(copy)

    own_routes.wait()
    for peer in order[1:]:
        ref = group_routes.at[peer]
        pltpu.make_async_copy(ref, ref, route_recv.at[peer]).wait()
    for i, plane in enumerate(planes):
        copy = pltpu.make_async_remote_copy(
            src_ref=group_routes,
            dst_ref=every_routes.at[here],
            send_sem=far_send.at[i],
            recv_sem=far_recv.at[here],
            device_id={"ep": plane},
        )
        copy.start()
        pending.append(copy)

    if relay:
        gather(0, 0)
        landed(sib, 0)
        landed(sib, 1)
        gather(1, 1)
        landed(nx, 0)
        send(blocks.at[nx], 0, nx, ny, 6)
        send(blocks.at[nx], 0, nx, sib, 7)
        landed(ny, 1)
        send(blocks.at[ny], 1, ny, nx, 8)
        send(blocks.at[ny], 1, ny, sib, 9)
        for copy in weights[:3]:
            copy.wait()
        expert([0, 1])
        landed(nx, 1)
        send(blocks.at[nx], 1, nx, sib, 10)
        landed(ny, 0)
        send(blocks.at[ny], 0, ny, sib, 11)
        gather(2, 0)
        gather(4, 1)
        expert([2, 4])
        for i, at in ((3, 0), (5, 1)):
            landed(order[i], 0)
            landed(order[i], 1)
            gather(i, at)
        expert([3, 5])
        landed(nd, 0)
        send(blocks.at[nd], 0, nd, sib, 12)
        landed(nd, 1)
        send(blocks.at[nd], 1, nd, sib, 13)
        gather(6, 0)
        landed(order[7], 0)
        landed(order[7], 1)
        gather(7, 1)
        expert([6, 7])
    else:
        for copy in weights[:3]:
            copy.wait()
        for number in range(n // chunk):
            members = list(range(number * chunk, (number + 1) * chunk))
            for i in members:
                if i > 0:
                    landed(order[i], 0)
                    landed(order[i], 1)
                gather(i, i % chunk)
            expert(members)

    for copy in weights[3:]:
        copy.wait()
    rows_in[:rows] = normed_of(tokens[...].astype(F32))
    shared = gated(rows_in[:rows], s_gate, s_up)
    for at in range(0, width, tile):
        total[:, at : at + tile] = jnp.dot(
            shared, s_down[:, at : at + tile], preferred_element_type=F32
        )

    expert_ids = lax.broadcasted_iota(jnp.int32, (n, rows), 0)
    first, second = routes[0:1], routes[1:2]
    member = ((first == expert_ids) | (second == expert_ids)).astype(F32)
    ranks = jnp.dot(member.astype(BF16), earlier, preferred_element_type=F32)
    slots = [
        named * cap
        + jnp.sum(jnp.where(named == expert_ids, ranks, 0.0), axis=0, keepdims=True).astype(jnp.int32)
        for named in (first, second)
    ]

    def counted(ref_of, amount, start):
        def step(i, sums):
            named = ref_of(i)
            return (
                sums
                + (named[0:1] == expert_ids).astype(F32)
                + (named[1:2] == expert_ids).astype(F32)
            )

        return lax.fori_loop(0, amount, step, start)

    sums = counted(lambda i: group_routes[i], n, jnp.zeros((n, rows), F32))
    for plane in planes:
        ref = every_routes.at[plane]
        pltpu.make_async_copy(ref, ref, far_recv.at[plane]).wait()
        sums = counted(lambda i, plane=plane: every_routes[plane, i], n, sums)
    counts = lax.dot_general(
        jnp.ones((8, rows), F32),
        sums,
        (((1,), (1,)), ((), ())),
        precision=lax.Precision.HIGHEST,
        preferred_element_type=F32,
    )
    load[...] = counts[0:1, :] * (n / (rows * 2 * n * eps))

    columns = jnp.transpose(jnp.broadcast_to(gates[0:1], (8, rows))), jnp.transpose(
        jnp.broadcast_to(gates[1:2], (8, rows))
    )
    gate_of = [column[:, 0:1] for column in columns]
    if relay:
        parts = [[0, 1], [2, 4], [3, 5], [6], [7]]
    else:
        parts = [list(range(at, at + chunk)) for at in range(0, n, chunk)]
    for members in parts:
        sources = [order[i] for i in members]
        picks = [
            jnp.transpose(
                jnp.concatenate(
                    [(row_in_slot + source * cap == slot).astype(F32) for source in sources], axis=0
                )
            ).astype(BF16)
            for slot in slots
        ]
        for i, source in zip(members, sources):
            if i > 0:
                ref = returned.at[source]
                pltpu.make_async_copy(ref, ref, result_recv.at[source]).wait()
        last = members is parts[-1]
        for at in range(0, width, tile):
            back = jnp.concatenate([returned[source, :, at : at + tile] for source in sources], axis=0)
            value = total[:, at : at + tile]
            for k in range(2):
                value = value + gate_of[k] * jnp.dot(picks[k], back, preferred_element_type=F32)
            if last:
                out[:, at : at + tile] = value.astype(BF16)
            else:
                total[:, at : at + tile] = value

    for copy in pending:
        copy.wait_send()


def write_out(mixed, load, mixed_out, load_out, sem):
    copies = [
        pltpu.make_async_copy(mixed, mixed_out, sem.at[0]),
        pltpu.make_async_copy(load, load_out, sem.at[1]),
    ]
    for copy in copies:
        copy.start()
    for copy in copies:
        copy.wait()


def per_device(
    tokens,
    norm_gain,
    routes,
    gates,
    expert_gate,
    expert_up,
    expert_down,
    shared_gate,
    shared_up,
    shared_down,
):
    n, eps = lax.axis_size("tp"), lax.axis_size("ep")
    rows, width = tokens.shape
    top = routes.shape[1]
    cap = 2 * rows * top // n
    units = expert_gate.shape[2]
    sends = 14 if n == 8 else 2 * (n - 1)
    vmem = pl.BlockSpec(memory_space=pltpu.VMEM)
    hbm = pl.BlockSpec(memory_space=pl.ANY)
    dma = pltpu.SemaphoreType.DMA
    mixed, load = pl.pallas_call(
        functools.partial(kernel, n, eps, cap),
        out_shape=(
            pltpu.VMEM((rows, width), BF16),
            pltpu.VMEM((1, n), F32),
        ),
        in_specs=[hbm] + [vmem] * 3 + [hbm] * 6,
        out_specs=(vmem, vmem),
        scratch_shapes=[
            pltpu.VMEM((rows, width), BF16),
            pltpu.VMEM((n, rows, width), BF16),
            pltpu.VMEM((n, top, rows), jnp.int32),
            pltpu.VMEM((eps, n, top, rows), jnp.int32),
            pltpu.VMEM((rows, width), BF16),
            pltpu.VMEM((rows, units), BF16),
            pltpu.VMEM((n, cap, width), BF16),
            pltpu.VMEM((n, cap, width), BF16),
            pltpu.VMEM((rows, width), F32),
            pltpu.VMEM(expert_gate.shape[1:], BF16),
            pltpu.VMEM(expert_up.shape[1:], BF16),
            pltpu.VMEM(expert_down.shape[1:], BF16),
            pltpu.VMEM(shared_gate.shape, BF16),
            pltpu.VMEM(shared_up.shape, BF16),
            pltpu.VMEM(shared_down.shape, BF16),
            dma((6,)),
            dma((2,)),
            dma((n - 1,)),
            dma((n,)),
            dma((max(1, eps - 1),)),
            dma((eps,)),
            dma((sends,)),
            dma((n, 2)),
            dma((n,)),
            dma((n,)),
        ],
        compiler_params=pltpu.CompilerParams(
            collective_id=0, has_side_effects=True
        ),
    )(
        tokens,
        routes.T,
        gates.T,
        norm_gain.reshape(1, width),
        expert_gate,
        expert_up,
        expert_down,
        shared_gate,
        shared_up,
        shared_down,
    )
    mixed, load = pl.pallas_call(
        write_out,
        out_shape=(
            jax.ShapeDtypeStruct((rows, width), BF16),
            jax.ShapeDtypeStruct((1, n), F32),
        ),
        in_specs=[vmem] * 2,
        out_specs=(hbm, hbm),
        scratch_shapes=[dma((2,))],
        compiler_params=pltpu.CompilerParams(vmem_limit_bytes=1 << 20),
    )(mixed, load)
    return mixed, load.reshape(n)


def solution(mesh):
    placed = (
        P(("ep", "tp"), None),
        P(),
        P(("ep", "tp"), None),
        P(("ep", "tp"), None),
        P("tp", None, None),
        P("tp", None, None),
        P("tp", None, None),
        P(),
        P(),
        P(),
    )
    return jax.shard_map(
        per_device,
        mesh=mesh,
        in_specs=placed,
        out_specs=(P(("ep", "tp"), None), P()),
        check_vma=False,
    )
```

profile of v0, /device:TPU:0, one launch (start us, length us, event | category | flops | bytes accessed | tf_op | source)
XLA Modules:
  0.0 49.8 jit_solution(12965407211597116402)
XLA Ops:
  0.6 48.4 %shard_map.113 = (bf16[128,2048]{1,0:T(8,128)(2,1)S(1)}, f32[1,8]{1,0:T(1,128)S(1)}) custom-call(bf16[128,2048]{1,0:T(8,128)(2,1)} %tokens_hbm.1, s32[2,128]{1,0:T(2,128)} %bitcast.5, f32[2,128]{1,0:T(2,128)} %bitcast.6, f32[1,2048]{1,0:T(1,128)} %bitcast.4, bf16[1,2048,512]{2,1,0:T(8,128)(2,1)} %expert_gate.1, bf16[1,2048,512]{2,1,0:T(8,128)(2,1)} %expert_up.1, ...), custom_call_target="tpu_custom_call" | custom-call | tf_op jit(solution)/shard_map/pallas_call | solution.py:379
  49.0 0.8 %shard_map.114 = (bf16[128,2048]{1,0:T(8,128)(2,1)}, f32[1,8]{1,0:T(1,128)}) custom-call(bf16[128,2048]{1,0:T(8,128)(2,1)S(1)} %get-tuple-element.6.mixed, f32[1,8]{1,0:T(1,128)S(1)} %get-tuple-element.7.load), custom_call_target="tpu_custom_call" | custom-call | tf_op jit(solution)/shard_map/pallas_call | solution.py:429
where the time goes:
time: 50.4 us; the launch traced here: 49.8 us
  Pallas kernels  49.2 us (98%)
  between operations  0.64 us (1%)
    pallas_call x1, Pallas kernels, per_device(): pl.pallas_call(functools.partial(kernel, n, eps, cap), out_shape=(pltpu.V...  48.4 us

commit v1 on v0

--- a/solution.py
+++ b/solution.py
@@ -11,7 +11,7 @@
 BF16 = jnp.bfloat16
 
 
-def kernel(
+def direct(
     n,
     eps,
     cap,
@@ -58,16 +58,7 @@
     rows, width = tokens.shape
     half = rows // 2
     chunk = rows // cap
-    relay = n == 8
     order = [lax.rem(me + i, n) for i in range(n)]
-    if relay:
-        core, xbit, ybit = me % 2, (me // 2) % 2, me // 4
-        across = 1 - 2 * core
-        sib = me + across
-        nx = me + 2 * (1 - 2 * xbit)
-        ny = me + 4 * (1 - 2 * ybit)
-        nd = nx + 4 * (1 - 2 * ybit)
-        order = [me, sib, nx, nx + across, ny, ny + across, nd, nd + across]
 
     barrier = pltpu.get_barrier_semaphore()
     planes = [lax.rem(here + i, eps) for i in range(1, eps)]
@@ -129,17 +120,9 @@
         pltpu.make_async_copy(ref, ref, token_recv.at[slot, piece]).wait()
 
     own_tokens.wait()
-    if relay:
-        send(tokens, 0, me, nx, 0)
-        send(tokens, 1, me, ny, 1)
-        send(tokens, 1, me, nx, 2)
-        send(tokens, 0, me, ny, 3)
-        send(tokens, 0, me, sib, 4)
-        send(tokens, 1, me, sib, 5)
-    else:
-        for i, peer in enumerate(order[1:]):
-            send(tokens, 0, me, peer, 2 * i)
-            send(tokens, 1, me, peer, 2 * i + 1)
+    for i, peer in enumerate(order[1:]):
+        send(tokens, 0, me, peer, 2 * i)
+        send(tokens, 1, me, peer, 2 * i + 1)
 
     earlier = (
         lax.broadcasted_iota(jnp.int32, (rows, rows), 0)
@@ -216,52 +199,16 @@
         copy.start()
         pending.append(copy)
 
-    if relay:
-        gather(0, 0)
-        landed(sib, 0)
-        landed(sib, 1)
-        gather(1, 1)
-        landed(nx, 0)
-        send(blocks.at[nx], 0, nx, ny, 6)
-        send(blocks.at[nx], 0, nx, sib, 7)
-        landed(ny, 1)
-        send(blocks.at[ny], 1, ny, nx, 8)
-        send(blocks.at[ny], 1, ny, sib, 9)
-        for copy in weights[:3]:
-            copy.wait()
-        expert([0, 1])
-        landed(nx, 1)
-        send(blocks.at[nx], 1, nx, sib, 10)
-        landed(ny, 0)
-        send(blocks.at[ny], 0, ny, sib, 11)
-        gather(2, 0)
-        gather(4, 1)
-        expert([2, 4])
-        for i, at in ((3, 0), (5, 1)):
-            landed(order[i], 0)
-            landed(order[i], 1)
-            gather(i, at)
-        expert([3, 5])
-        landed(nd, 0)
-        send(blocks.at[nd], 0, nd, sib, 12)
-        landed(nd, 1)
-        send(blocks.at[nd], 1, nd, sib, 13)
-        gather(6, 0)
-        landed(order[7], 0)
-        landed(order[7], 1)
-        gather(7, 1)
-        expert([6, 7])
-    else:
-        for copy in weights[:3]:
-            copy.wait()
-        for number in range(n // chunk):
-            members = list(range(number * chunk, (number + 1) * chunk))
-            for i in members:
-                if i > 0:
-                    landed(order[i], 0)
-                    landed(order[i], 1)
-                gather(i, i % chunk)
-            expert(members)
+    for copy in weights[:3]:
+        copy.wait()
+    for number in range(n // chunk):
+        members = list(range(number * chunk, (number + 1) * chunk))
+        for i in members:
+            if i > 0:
+                landed(order[i], 0)
+                landed(order[i], 1)
+            gather(i, i % chunk)
+        expert(members)
 
     for copy in weights[3:]:
         copy.wait()
@@ -311,10 +258,7 @@
         jnp.broadcast_to(gates[1:2], (8, rows))
     )
     gate_of = [column[:, 0:1] for column in columns]
-    if relay:
-        parts = [[0, 1], [2, 4], [3, 5], [6], [7]]
-    else:
-        parts = [list(range(at, at + chunk)) for at in range(0, n, chunk)]
+    parts = [list(range(at, at + chunk)) for at in range(0, n, chunk)]
     for members in parts:
         sources = [order[i] for i in members]
         picks = [
@@ -344,6 +288,439 @@
         copy.wait_send()
 
 
+def square(
+    eps,
+    tokens_hbm,
+    routes,
+    gates,
+    gain,
+    expert_gate,
+    expert_up,
+    expert_down,
+    shared_gate,
+    shared_up,
+    shared_down,
+    out,
+    load,
+    blocks,
+    group_routes,
+    every_routes,
+    near_gates,
+    lanes,
+    columns,
+    normed,
+    hidden,
+    mine,
+    lent,
+    theirs,
+    shared,
+    merged,
+    passed,
+    back,
+    base,
+    w_gate,
+    w_up,
+    w_down,
+    s_gate,
+    s_up,
+    s_down,
+    weight_sem,
+    own_sem,
+    route_send,
+    route_recv,
+    far_send,
+    far_recv,
+    gate_recv,
+    sent,
+    token_recv,
+    core_recv,
+    result_recv,
+    passed_recv,
+    back_recv,
+):
+    n = 8
+    me = lax.axis_index("tp")
+    here = lax.axis_index("ep")
+    rows, width = out.shape
+    half, quarter = rows // 2, rows // 4
+    piece = 16
+    steps = half // piece
+    core, xbit, ybit = me % 2, (me // 2) % 2, me // 4
+    across = 1 - 2 * core
+    sib = me + across
+    nx = me + 2 * (1 - 2 * xbit)
+    ny = me + 4 * (1 - 2 * ybit)
+    nd = nx + 4 * (1 - 2 * ybit)
+    others = [sib, nx, ny, nd, nx + across, ny + across, nd + across]
+
+    barrier = pltpu.get_barrier_semaphore()
+    planes = [lax.rem(here + i, eps) for i in range(1, eps)]
+    for peer in others:
+        pl.semaphore_signal(barrier, inc=1, device_id={"tp": peer})
+    for plane in planes:
+        pl.semaphore_signal(barrier, inc=1, device_id={"ep": plane})
+    own_tokens = pltpu.make_async_copy(tokens_hbm, blocks.at[0], own_sem.at[1])
+    own_tokens.start()
+    weights = [
+        pltpu.make_async_copy(src, dst, weight_sem.at[i])
+        for i, (src, dst) in enumerate(
+            [
+                (expert_gate.at[0], w_gate),
+                (expert_up.at[0], w_up),
+                (expert_down.at[0], w_down),
+                (shared_gate, s_gate),
+                (shared_up, s_up),
+                (shared_down, s_down),
+            ]
+        )
+    ]
+    for copy in weights:
+        copy.start()
+    own_routes = pltpu.make_async_copy(routes, group_routes.at[me], own_sem.at[0])
+    own_routes.start()
+
+    pl.semaphore_wait(barrier, n - 1 + eps - 1)
+
+    pending = []
+
+    def remote(source, target, send_sem, recv_sem, where):
+        copy = pltpu.make_async_remote_copy(
+            src_ref=source,
+            dst_ref=target,
+            send_sem=send_sem,
+            recv_sem=recv_sem,
+            device_id=where,
+        )
+        copy.start()
+        pending.append(copy)
+
+    numbers = iter(range(sent.shape[0]))
+
+    def send(source, target, recv_sem, peer):
+        remote(source, target, sent.at[next(numbers)], recv_sem, {"tp": peer})
+
+    def arrived(ref, sem):
+        pltpu.make_async_copy(ref, ref, sem).wait()
+
+    def at_rows(ref, start, size):
+        return ref.at[pl.ds(start, size)]
+
+    def token_send(source, start, size, group, number, peer):
+        send(
+            at_rows(blocks.at[source], start, size),
+            at_rows(blocks.at[group], start, size),
+            token_recv.at[group, number],
+            peer,
+        )
+
+    def lend(group, start, size, number):
+        send(
+            at_rows(blocks.at[group], start, size),
+            at_rows(blocks.at[group + 4], start, size),
+            core_recv.at[group, number],
+            sib,
+        )
+
+    def landed(group, start, size, number):
+        arrived(at_rows(blocks.at[group], start, size), token_recv.at[group, number])
+        lend(group, start, size, number)
+
+    def lent_in(group, start, size, number):
+        arrived(at_rows(blocks.at[group + 4], start, size), core_recv.at[group, number])
+
+    for i, peer in enumerate(others):
+        remote(routes, group_routes.at[me], route_send.at[i], route_recv.at[me], {"tp": peer})
+    for i, peer in enumerate([nx, ny, nd]):
+        send(gates, near_gates.at[i], gate_recv.at[i], peer)
+    own_tokens.wait()
+    token_send(0, 0, half, 1, 0, nx)
+    token_send(0, half, half, 1, 1, ny)
+    token_send(0, half, quarter, 2, 2, nx)
+    token_send(0, 0, quarter, 2, 0, ny)
+    lend(0, 0, rows, 0)
+
+    def norm(group):
+        values = blocks[group].astype(F32)
+        center = jnp.mean(values, axis=-1, keepdims=True)
+        values = values - center
+        spread = jnp.mean(jnp.square(values), axis=-1, keepdims=True)
+        normed[...] = (values * lax.rsqrt(spread + 1e-05) * gain[...]).astype(BF16)
+
+    def gated(values, gate_ref, up_ref):
+        gate_part = jnp.dot(values, gate_ref[...], preferred_element_type=F32)
+        up_part = jnp.dot(values, up_ref[...], preferred_element_type=F32)
+        return (gate_part * (1.0 / (1.0 + jnp.exp(-gate_part))) * up_part).astype(BF16)
+
+    tile = 512
+
+    def expert(result):
+        hidden[...] = gated(normed[...], w_gate, w_up)
+        for at in range(0, width, tile):
+            result[:, at : at + tile] = jnp.dot(
+                hidden[...], w_down[:, at : at + tile], preferred_element_type=F32
+            ).astype(BF16)
+
+    def common(group):
+        inner = gated(normed[...], s_gate, s_up)
+        for at in range(0, width, tile):
+            shared[group, :, at : at + tile] = jnp.dot(
+                inner, s_down[:, at : at + tile], preferred_element_type=F32
+            )
+
+    def serve(group):
+        norm(group + 4)
+        expert(lent.at[group])
+        send(lent.at[group], theirs.at[group], result_recv.at[group], sib)
+
+    def named(ids):
+        def test(route):
+            hit = route == ids[0]
+            for one in ids[1:]:
+                hit = hit | (route == one)
+            return hit
+
+        return test
+
+    def share(route, gate, test):
+        first, second = test(route[0:1]), test(route[1:2])
+        amount = first.astype(F32) + second.astype(F32)
+        weight = jnp.where(first, gate[0:1], jnp.where(second, gate[1:2], 0.0))
+        return amount, weight
+
+    def store_columns(group, values):
+        for i, value in enumerate(values):
+            lanes[group, i : i + 1] = value
+        columns[group] = jnp.transpose(lanes[group])
+
+    lane = lax.broadcasted_iota(jnp.int32, (2, rows), 1)
+    low = lane < half
+    low_row = low[0:1]
+    is_me, is_sib = named([me]), named([sib])
+    on_x, on_y = named([nx, nx + across]), named([ny, ny + across])
+    on_xd = named([nx, nx + across, nd, nd + across])
+    on_yd = named([ny, ny + across, nd, nd + across])
+
+    def coefficients(group, route, gate, relayed=False):
+        mine_n, mine_g = share(route, gate, is_me)
+        sib_n, sib_g = share(route, gate, is_sib)
+        both = mine_n + sib_n
+        if relayed:
+            by_x, by_y = share(route, gate, on_x), share(route, gate, on_y)
+            far_n, far_g = [jnp.where(low_row, a, b) for a, b in zip(by_x, by_y)]
+            full = (both + far_n == 2.0) & (far_n < 2.0)
+        else:
+            full = both == 2.0
+        values = [
+            jnp.where(full, mine_g, mine_n),
+            jnp.where(full, sib_g, sib_n),
+            full.astype(F32),
+        ]
+        if relayed:
+            values.append(jnp.where(full, far_g, 1.0))
+        store_columns(group, values)
+
+    def own_coefficients():
+        route, gate = routes[...], gates[...]
+        _, mine_g = share(route, gate, is_me)
+        _, sib_g = share(route, gate, is_sib)
+        x_low, x_high = share(route, gate, on_x), share(route, gate, on_xd)
+        y_low, y_high = share(route, gate, on_yd), share(route, gate, on_y)
+        x_n, x_g = [jnp.where(low_row, a, b) for a, b in zip(x_low, x_high)]
+        y_n, y_g = [jnp.where(low_row, a, b) for a, b in zip(y_low, y_high)]
+        done_x, done_y = x_n == 2.0, y_n == 2.0
+        store_columns(
+            0,
+            [
+                mine_g,
+                sib_g,
+                jnp.where(done_x | done_y, 0.0, 1.0),
+                jnp.where(done_x, 1.0, x_g),
+                jnp.where(done_y, 1.0, y_g),
+            ],
+        )
+
+    def column(group, i, start, size):
+        return columns[group, pl.ds(start, size), i : i + 1]
+
+    def local_sum(group, start, size):
+        where = pl.ds(start, size)
+        return (
+            column(group, 0, start, size) * mine[group, where].astype(F32)
+            + column(group, 1, start, size) * theirs[group, where].astype(F32)
+            + column(group, 2, start, size) * shared[group, where]
+        )
+
+    def into_sum(total, group):
+        def step(i, carry):
+            start = pl.multiple_of(i * piece, piece)
+            total[pl.ds(start, piece)] = local_sum(group, start, piece)
+            return carry
+
+        lax.fori_loop(0, rows // piece, step, 0)
+
+    def merge(group):
+        def step(i, carry):
+            start = pl.multiple_of(i * piece, piece)
+            merged[group, pl.ds(start, piece)] = local_sum(group, start, piece).astype(BF16)
+            return carry
+
+        lax.fori_loop(0, rows // piece, step, 0)
+
+    norm(0)
+    for copy in weights[:3]:
+        copy.wait()
+    expert(mine.at[0])
+    for copy in weights[3:]:
+        copy.wait()
+    common(0)
+    lent_in(0, 0, rows, 0)
+    serve(0)
+
+    own_routes.wait()
+    for peer in others:
+        arrived(group_routes.at[peer], route_recv.at[peer])
+    for i in range(3):
+        arrived(near_gates.at[i], gate_recv.at[i])
+    for i, plane in enumerate(planes):
+        remote(group_routes, every_routes.at[here], far_send.at[i], far_recv.at[here], {"ep": plane})
+
+    landed(1, 0, half, 0)
+    token_send(1, 0, half, 3, 0, ny)
+    landed(1, half, half, 1)
+    token_send(1, half, half, 3, 1, nx)
+    token_send(0, half + quarter, quarter, 2, 3, nx)
+    token_send(0, quarter, quarter, 2, 1, ny)
+    own_coefficients()
+    x_route, y_route, d_route = group_routes[nx], group_routes[ny], group_routes[nd]
+    x_gate, y_gate, d_gate = near_gates[0], near_gates[1], near_gates[2]
+    coefficients(1, jnp.where(low, x_route, y_route), jnp.where(low, x_gate, y_gate))
+    norm(1)
+    expert(mine.at[1])
+    common(1)
+    lent_in(1, 0, half, 0)
+    lent_in(1, half, half, 1)
+    serve(1)
+    landed(2, half, quarter, 2)
+    landed(2, 0, quarter, 0)
+
+    arrived(theirs.at[1], result_recv.at[1])
+    merge(1)
+    for first, peer in ((0, nx), (1, ny)):
+        send(
+            at_rows(merged.at[1], first * half, half),
+            at_rows(back.at[first], first * half, half),
+            back_recv.at[first, steps],
+            peer,
+        )
+    coefficients(3, d_route, d_gate)
+    coefficients(
+        2,
+        jnp.where(low, y_route, x_route),
+        jnp.where(low, y_gate, x_gate),
+        relayed=True,
+    )
+    arrived(theirs.at[0], result_recv.at[0])
+    into_sum(base, 0)
+
+    landed(3, 0, half, 0)
+    landed(3, half, half, 1)
+    norm(3)
+    expert(mine.at[3])
+    common(3)
+    lent_in(3, 0, half, 0)
+    lent_in(3, half, half, 1)
+    serve(3)
+    landed(2, half + quarter, quarter, 3)
+    landed(2, quarter, quarter, 1)
+    arrived(theirs.at[3], result_recv.at[3])
+    merge(3)
+    for step in range(steps):
+        for first, peer in ((0, nx), (1, ny)):
+            start = first * half + step * piece
+            send(
+                at_rows(merged.at[3], start, piece),
+                at_rows(passed, start, piece),
+                passed_recv.at[first, step],
+                peer,
+            )
+    norm(2)
+    expert(mine.at[2])
+    common(2)
+    for number in range(4):
+        lent_in(2, number * quarter, quarter, number)
+    serve(2)
+
+    expert_ids = lax.broadcasted_iota(jnp.int32, (n, rows), 0)
+
+    def counted(ref_of, amount, start):
+        def step(i, sums):
+            route = ref_of(i)
+            return (
+                sums
+                + (route[0:1] == expert_ids).astype(F32)
+                + (route[1:2] == expert_ids).astype(F32)
+            )
+
+        return lax.fori_loop(0, amount, step, start)
+
+    sums = counted(lambda i: group_routes[i], n, jnp.zeros((n, rows), F32))
+    for plane in planes:
+        arrived(every_routes.at[plane], far_recv.at[plane])
+        sums = counted(lambda i, plane=plane: every_routes[plane, i], n, sums)
+    counts = lax.dot_general(
+        jnp.ones((8, rows), F32),
+        sums,
+        (((1,), (1,)), ((), ())),
+        precision=lax.Precision.HIGHEST,
+        preferred_element_type=F32,
+    )
+    load[...] = counts[0:1, :] * (n / (rows * 2 * n * eps))
+
+    arrived(theirs.at[2], result_recv.at[2])
+    into_sum(shared.at[2], 2)
+
+    for step in range(steps):
+        for first, peer in ((1, nx), (0, ny)):
+            start = first * half + step * piece
+            where = pl.ds(start, piece)
+            arrived(at_rows(passed, start, piece), passed_recv.at[first, step])
+            merged[2, where] = (
+                shared[2, where] + column(2, 3, start, piece) * passed[where].astype(F32)
+            ).astype(BF16)
+            send(
+                at_rows(merged.at[2], start, piece),
+                at_rows(back.at[1 - first], start, piece),
+                back_recv.at[1 - first, step],
+                peer,
+            )
+
+    for first in range(2):
+        arrived(at_rows(back.at[first], first * half, half), back_recv.at[first, steps])
+
+    def early(i, carry):
+        for first in range(2):
+            start = pl.multiple_of(first * half + i * piece, piece)
+            where = pl.ds(start, piece)
+            base[where] = base[where] + column(0, 3 + first, start, piece) * back[
+                first, where
+            ].astype(F32)
+        return carry
+
+    lax.fori_loop(0, steps, early, 0)
+
+    for step in range(steps):
+        for first in range(2):
+            start = (1 - first) * half + step * piece
+            where = pl.ds(start, piece)
+            arrived(at_rows(back.at[first], start, piece), back_recv.at[first, step])
+            out[where] = (
+                base[where] + column(0, 3 + first, start, piece) * back[first, where].astype(F32)
+            ).astype(BF16)
+
+    for copy in pending:
+        copy.wait_send()
+
+
 def write_out(mixed, load, mixed_out, load_out, sem):
     copies = [
         pltpu.make_async_copy(mixed, mixed_out, sem.at[0]),
@@ -372,19 +749,54 @@
     top = routes.shape[1]
     cap = 2 * rows * top // n
     units = expert_gate.shape[2]
-    sends = 14 if n == 8 else 2 * (n - 1)
     vmem = pl.BlockSpec(memory_space=pltpu.VMEM)
     hbm = pl.BlockSpec(memory_space=pl.ANY)
     dma = pltpu.SemaphoreType.DMA
-    mixed, load = pl.pallas_call(
-        functools.partial(kernel, n, eps, cap),
-        out_shape=(
+    weights = [
+        pltpu.VMEM(expert_gate.shape[1:], BF16),
+        pltpu.VMEM(expert_up.shape[1:], BF16),
+        pltpu.VMEM(expert_down.shape[1:], BF16),
+        pltpu.VMEM(shared_gate.shape, BF16),
+        pltpu.VMEM(shared_up.shape, BF16),
+        pltpu.VMEM(shared_down.shape, BF16),
+        dma((6,)),
+        dma((2,)),
+        dma((n - 1,)),
+        dma((n,)),
+        dma((max(1, eps - 1),)),
+        dma((eps,)),
+    ]
+    if n == 8:
+        body = functools.partial(square, eps)
+        scratch = [
+            pltpu.VMEM((8, rows, width), BF16),
+            pltpu.VMEM((n, top, rows), jnp.int32),
+            pltpu.VMEM((eps, n, top, rows), jnp.int32),
+            pltpu.VMEM((3, top, rows), F32),
+            pltpu.VMEM((4, 8, rows), F32),
+            pltpu.VMEM((4, rows, 8), F32),
             pltpu.VMEM((rows, width), BF16),
-            pltpu.VMEM((1, n), F32),
-        ),
-        in_specs=[hbm] + [vmem] * 3 + [hbm] * 6,
-        out_specs=(vmem, vmem),
-        scratch_shapes=[
+            pltpu.VMEM((rows, units), BF16),
+            pltpu.VMEM((4, rows, width), BF16),
+            pltpu.VMEM((4, rows, width), BF16),
+            pltpu.VMEM((4, rows, width), BF16),
+            pltpu.VMEM((4, rows, width), F32),
+            pltpu.VMEM((4, rows, width), BF16),
+            pltpu.VMEM((rows, width), BF16),
+            pltpu.VMEM((2, rows, width), BF16),
+            pltpu.VMEM((rows, width), F32),
+            *weights,
+            dma((3,)),
+            dma((26 + rows // 8,)),
+            dma((4, 4)),
+            dma((4, 4)),
+            dma((4,)),
+            dma((2, rows // 32)),
+            dma((2, rows // 32 + 1)),
+        ]
+    else:
+        body = functools.partial(direct, n, eps, cap)
+        scratch = [
             pltpu.VMEM((rows, width), BF16),
             pltpu.VMEM((n, rows, width), BF16),
             pltpu.VMEM((n, top, rows), jnp.int32),
@@ -394,23 +806,21 @@
             pltpu.VMEM((n, cap, width), BF16),
             pltpu.VMEM((n, cap, width), BF16),
             pltpu.VMEM((rows, width), F32),
-            pltpu.VMEM(expert_gate.shape[1:], BF16),
-            pltpu.VMEM(expert_up.shape[1:], BF16),
-            pltpu.VMEM(expert_down.shape[1:], BF16),
-            pltpu.VMEM(shared_gate.shape, BF16),
-            pltpu.VMEM(shared_up.shape, BF16),
-            pltpu.VMEM(shared_down.shape, BF16),
-            dma((6,)),
-            dma((2,)),
-            dma((n - 1,)),
-            dma((n,)),
-            dma((max(1, eps - 1),)),
-            dma((eps,)),
-            dma((sends,)),
+            *weights,
+            dma((2 * (n - 1),)),
             dma((n, 2)),
             dma((n,)),
             dma((n,)),
-        ],
+        ]
+    mixed, load = pl.pallas_call(
+        body,
+        out_shape=(
+            pltpu.VMEM((rows, width), BF16),
+            pltpu.VMEM((1, n), F32),
+        ),
+        in_specs=[hbm] + [vmem] * 3 + [hbm] * 6,
+        out_specs=(vmem, vmem),
+        scratch_shapes=scratch,
         compiler_params=pltpu.CompilerParams(
             collective_id=0, has_side_effects=True
         ),

time: 50.4 us -> 45.8 us (0.909)
  Pallas kernels: 49.2 us -> 44.7 us
    pallas_call x1, Pallas kernels: 48.4 us -> 43.9 us  [per_device(): pl.pallas_call(body, out_shape=(pltpu.VMEM((rows, width), BF16), pltpu.VM...]
where the time goes in v1:
time: 45.8 us; the launch traced here: 45.5 us
  Pallas kernels  44.7 us (98%)
  between operations  0.8 us (2%)
    pallas_call x1, Pallas kernels, per_device(): pl.pallas_call(body, out_shape=(pltpu.VMEM((rows, width), BF16), pltpu.VM...  43.9 us

profile of v1, /device:TPU:0, one launch (start us, length us, event | category | flops | bytes accessed | tf_op | source)
XLA Modules:
  0.0 45.5 jit_solution(5006745201304424779)
XLA Ops:
  0.6 43.9 %shard_map.113 = (bf16[128,2048]{1,0:T(8,128)(2,1)S(1)}, f32[1,8]{1,0:T(1,128)S(1)}) custom-call(bf16[128,2048]{1,0:T(8,128)(2,1)} %tokens_hbm.1, s32[2,128]{1,0:T(2,128)} %bitcast.5, f32[2,128]{1,0:T(2,128)} %bitcast.6, f32[1,2048]{1,0:T(1,128)} %bitcast.4, bf16[1,2048,512]{2,1,0:T(8,128)(2,1)} %expert_gate.1, bf16[1,2048,512]{2,1,0:T(8,128)(2,1)} %expert_up.1, ...), custom_call_target="tpu_custom_call" | custom-call | tf_op jit(solution)/shard_map/pallas_call | solution.py:815
  44.6 0.8 %shard_map.114 = (bf16[128,2048]{1,0:T(8,128)(2,1)}, f32[1,8]{1,0:T(1,128)}) custom-call(bf16[128,2048]{1,0:T(8,128)(2,1)S(1)} %get-tuple-element.6.mixed, f32[1,8]{1,0:T(1,128)S(1)} %get-tuple-element.7.load), custom_call_target="tpu_custom_call" | custom-call | tf_op jit(solution)/shard_map/pallas_call | solution.py:839

commit v2 on v1

--- a/solution.py
+++ b/solution.py
@@ -291,9 +291,9 @@
 def square(
     eps,
     tokens_hbm,
-    routes,
-    gates,
-    gain,
+    routes_hbm,
+    gates_hbm,
+    gain_hbm,
     expert_gate,
     expert_up,
     expert_down,
@@ -303,9 +303,12 @@
     out,
     load,
     blocks,
-    group_routes,
-    every_routes,
+    routes,
+    gates,
+    gain,
+    near_routes,
     near_gates,
+    tally,
     lanes,
     columns,
     normed,
@@ -318,20 +321,14 @@
     passed,
     back,
     base,
-    w_gate,
-    w_up,
+    w_in,
     w_down,
-    s_gate,
-    s_up,
+    s_in,
     s_down,
-    weight_sem,
     own_sem,
-    route_send,
-    route_recv,
-    far_send,
-    far_recv,
-    gate_recv,
     sent,
+    meta_recv,
+    tally_recv,
     token_recv,
     core_recv,
     result_recv,
@@ -351,100 +348,147 @@
     nx = me + 2 * (1 - 2 * xbit)
     ny = me + 4 * (1 - 2 * ybit)
     nd = nx + 4 * (1 - 2 * ybit)
-    others = [sib, nx, ny, nd, nx + across, ny + across, nd + across]
+    column_head = me == 0
+    below, above = column_head & (here > 0), column_head & (here < eps - 1)
 
     barrier = pltpu.get_barrier_semaphore()
-    planes = [lax.rem(here + i, eps) for i in range(1, eps)]
-    for peer in others:
+    for peer in (sib, nx, ny):
         pl.semaphore_signal(barrier, inc=1, device_id={"tp": peer})
-    for plane in planes:
-        pl.semaphore_signal(barrier, inc=1, device_id={"ep": plane})
-    own_tokens = pltpu.make_async_copy(tokens_hbm, blocks.at[0], own_sem.at[1])
-    own_tokens.start()
-    weights = [
-        pltpu.make_async_copy(src, dst, weight_sem.at[i])
-        for i, (src, dst) in enumerate(
-            [
-                (expert_gate.at[0], w_gate),
-                (expert_up.at[0], w_up),
-                (expert_down.at[0], w_down),
-                (shared_gate, s_gate),
-                (shared_up, s_up),
-                (shared_down, s_down),
-            ]
-        )
+
+    @pl.when(below)
+    def _():
+        pl.semaphore_signal(barrier, inc=1, device_id={"ep": here - 1})
+
+    @pl.when(above)
+    def _():
+        pl.semaphore_signal(barrier, inc=1, device_id={"ep": here + 1})
+
+    copies = [
+        (0, tokens_hbm, blocks.at[0]),
+        (1, routes_hbm, routes),
+        (2, gates_hbm, gates),
+        (3, gain_hbm, gain),
+        (4, expert_gate.at[0], w_in.at[0]),
+        (4, expert_up.at[0], w_in.at[1]),
+        (5, expert_down.at[0], w_down),
+        (6, shared_gate, s_in.at[0]),
+        (6, shared_up, s_in.at[1]),
+        (7, shared_down, s_down),
     ]
-    for copy in weights:
-        copy.start()
-    own_routes = pltpu.make_async_copy(routes, group_routes.at[me], own_sem.at[0])
-    own_routes.start()
-
-    pl.semaphore_wait(barrier, n - 1 + eps - 1)
-
-    pending = []
-
-    def remote(source, target, send_sem, recv_sem, where):
-        copy = pltpu.make_async_remote_copy(
+    for number, source, target in copies:
+        pltpu.make_async_copy(source, target, own_sem.at[number]).start()
+
+    def arrived(ref, sem):
+        pltpu.make_async_copy(ref, ref, sem).wait()
+
+    pl.semaphore_wait(barrier, 3 + jnp.where(below, 1, 0) + jnp.where(above, 1, 0))
+
+    def send(source, target, send_sem, recv_sem, where):
+        pltpu.make_async_remote_copy(
             src_ref=source,
             dst_ref=target,
             send_sem=send_sem,
             recv_sem=recv_sem,
             device_id=where,
-        )
-        copy.start()
-        pending.append(copy)
-
-    numbers = iter(range(sent.shape[0]))
-
-    def send(source, target, recv_sem, peer):
-        remote(source, target, sent.at[next(numbers)], recv_sem, {"tp": peer})
-
-    def arrived(ref, sem):
-        pltpu.make_async_copy(ref, ref, sem).wait()
+        ).start()
 
     def at_rows(ref, start, size):
         return ref.at[pl.ds(start, size)]
 
+    def link(source, target, start, size, recv_sem, peer):
+        send(
+            at_rows(source, start, size),
+            at_rows(target, start, size),
+            sent.at[0],
+            recv_sem,
+            {"tp": peer},
+        )
+
     def token_send(source, start, size, group, number, peer):
-        send(
-            at_rows(blocks.at[source], start, size),
-            at_rows(blocks.at[group], start, size),
-            token_recv.at[group, number],
-            peer,
-        )
-
-    def lend(group, start, size, number):
+        link(blocks.at[source], blocks.at[group], start, size, token_recv.at[number], peer)
+
+    def lend(group, start, size):
         send(
             at_rows(blocks.at[group], start, size),
             at_rows(blocks.at[group + 4], start, size),
-            core_recv.at[group, number],
-            sib,
+            sent.at[1],
+            core_recv.at[group],
+            {"tp": sib},
         )
 
     def landed(group, start, size, number):
-        arrived(at_rows(blocks.at[group], start, size), token_recv.at[group, number])
-        lend(group, start, size, number)
-
-    def lent_in(group, start, size, number):
-        arrived(at_rows(blocks.at[group + 4], start, size), core_recv.at[group, number])
-
-    for i, peer in enumerate(others):
-        remote(routes, group_routes.at[me], route_send.at[i], route_recv.at[me], {"tp": peer})
-    for i, peer in enumerate([nx, ny, nd]):
-        send(gates, near_gates.at[i], gate_recv.at[i], peer)
-    own_tokens.wait()
+        arrived(at_rows(blocks.at[group], start, size), token_recv.at[number])
+
+    arrived(routes, own_sem.at[1])
+    arrived(gates, own_sem.at[2])
+    for i, peer in enumerate((nx, ny)):
+        send(routes, near_routes.at[i], sent.at[2], meta_recv.at[0], {"tp": peer})
+        send(gates, near_gates.at[i], sent.at[2], meta_recv.at[0], {"tp": peer})
+    arrived(blocks.at[0], own_sem.at[0])
     token_send(0, 0, half, 1, 0, nx)
     token_send(0, half, half, 1, 1, ny)
-    token_send(0, half, quarter, 2, 2, nx)
-    token_send(0, 0, quarter, 2, 0, ny)
-    lend(0, 0, rows, 0)
-
-    def norm(group):
+    lend(0, 0, rows)
+
+    expert_ids = lax.broadcasted_iota(jnp.int32, (n, rows), 0)
+
+    def tallied(route):
+        return (route[0:1] == expert_ids).astype(F32) + (route[1:2] == expert_ids).astype(F32)
+
+    def tally_send(source, target, number, recv, where):
+        send(tally.at[source], tally.at[target], sent.at[number], tally_recv.at[recv], where)
+
+    def along_column(rounds):
+        for r in rounds:
+
+            @pl.when(column_head & (here == r))
+            def _():
+                value = tally[2]
+                if r > 0:
+                    arrived(tally.at[3], tally_recv.at[1])
+                    value = value + tally[3]
+                tally[5] = value
+                if r < eps - 1:
+                    tally_send(5, 3, 5, 1, {"ep": here + 1})
+
+            @pl.when(column_head & (here == eps - 1 - r))
+            def _():
+                value = tally[2]
+                if r > 0:
+                    arrived(tally.at[4], tally_recv.at[2])
+                    value = value + tally[4]
+                tally[6] = value
+                if r < eps - 1:
+                    tally_send(6, 4, 6, 2, {"ep": here - 1})
+
+    hand = {
+        7: (core == 0, sib),
+        8: (column_head, nx),
+        9: ((core == 0) & (ybit == 0), ny),
+    }
+    handers = [
+        (column_head, (7, 8, 9)),
+        ((core == 0) & (xbit == 1) & (ybit == 0), (7, 9)),
+        ((core == 0) & (xbit == 0) & (ybit == 1), (7,)),
+        ((core == 0) & (xbit == 1) & (ybit == 1), (7,)),
+        (core == 1, ()),
+    ]
+
+    def hand_on(number):
+        test, numbers = handers[number]
+
+        @pl.when(test)
+        def _():
+            if number > 0:
+                arrived(tally.at[7], tally_recv.at[3])
+            for i in numbers:
+                tally_send(7, 7, i, 3, {"tp": hand[i][1]})
+
+    def norm(group, slot=0):
         values = blocks[group].astype(F32)
         center = jnp.mean(values, axis=-1, keepdims=True)
         values = values - center
         spread = jnp.mean(jnp.square(values), axis=-1, keepdims=True)
-        normed[...] = (values * lax.rsqrt(spread + 1e-05) * gain[...]).astype(BF16)
+        normed[slot] = (values * lax.rsqrt(spread + 1e-05) * gain[...]).astype(BF16)
 
     def gated(values, gate_ref, up_ref):
         gate_part = jnp.dot(values, gate_ref[...], preferred_element_type=F32)
@@ -453,24 +497,25 @@
 
     tile = 512
 
-    def expert(result):
-        hidden[...] = gated(normed[...], w_gate, w_up)
+    def expert(result, slot=0):
+        hidden[...] = gated(normed[slot], w_in.at[0], w_in.at[1])
         for at in range(0, width, tile):
             result[:, at : at + tile] = jnp.dot(
                 hidden[...], w_down[:, at : at + tile], preferred_element_type=F32
             ).astype(BF16)
 
     def common(group):
-        inner = gated(normed[...], s_gate, s_up)
+        inner = gated(normed[0], s_in.at[0], s_in.at[1])
         for at in range(0, width, tile):
             shared[group, :, at : at + tile] = jnp.dot(
                 inner, s_down[:, at : at + tile], preferred_element_type=F32
             )
 
     def serve(group):
-        norm(group + 4)
-        expert(lent.at[group])
-        send(lent.at[group], theirs.at[group], result_recv.at[group], sib)
+        arrived(blocks.at[group + 4], core_recv.at[group])
+        norm(group + 4, 1)
+        expert(lent.at[group], 1)
+        send(lent.at[group], theirs.at[group], sent.at[1], result_recv.at[group], {"tp": sib})
 
     def named(ids):
         def test(route):
@@ -558,144 +603,115 @@
 
         lax.fori_loop(0, rows // piece, step, 0)
 
-    def merge(group):
-        def step(i, carry):
-            start = pl.multiple_of(i * piece, piece)
-            merged[group, pl.ds(start, piece)] = local_sum(group, start, piece).astype(BF16)
-            return carry
-
-        lax.fori_loop(0, rows // piece, step, 0)
-
+    def merge(group, target_of, recv_of):
+        for step in range(steps):
+            for first, peer in ((0, nx), (1, ny)):
+                start = first * half + step * piece
+                merged[group, pl.ds(start, piece)] = local_sum(group, start, piece).astype(BF16)
+                link(merged.at[group], target_of(first), start, piece, recv_of(step), peer)
+
+    arrived(gain, own_sem.at[3])
     norm(0)
-    for copy in weights[:3]:
-        copy.wait()
+    arrived(w_in, own_sem.at[4])
+    arrived(w_down, own_sem.at[5])
     expert(mine.at[0])
-    for copy in weights[3:]:
-        copy.wait()
+    arrived(s_in, own_sem.at[6])
+    arrived(s_down, own_sem.at[7])
     common(0)
-    lent_in(0, 0, rows, 0)
     serve(0)
 
-    own_routes.wait()
-    for peer in others:
-        arrived(group_routes.at[peer], route_recv.at[peer])
-    for i in range(3):
-        arrived(near_gates.at[i], gate_recv.at[i])
-    for i, plane in enumerate(planes):
-        remote(group_routes, every_routes.at[here], far_send.at[i], far_recv.at[here], {"ep": plane})
-
-    landed(1, 0, half, 0)
-    token_send(1, 0, half, 3, 0, ny)
-    landed(1, half, half, 1)
-    token_send(1, half, half, 3, 1, nx)
-    token_send(0, half + quarter, quarter, 2, 3, nx)
-    token_send(0, quarter, quarter, 2, 1, ny)
+    arrived(tally.at[0], meta_recv.at[0])
+    arrived(tally.at[0], sent.at[2])
+    send(near_routes.at[0], near_routes.at[2], sent.at[3], meta_recv.at[1], {"tp": ny})
+    send(near_gates.at[0], near_gates.at[2], sent.at[3], meta_recv.at[1], {"tp": ny})
+    token_send(0, half, quarter, 2, 2, nx)
+    token_send(0, 0, quarter, 2, 2, ny)
     own_coefficients()
-    x_route, y_route, d_route = group_routes[nx], group_routes[ny], group_routes[nd]
-    x_gate, y_gate, d_gate = near_gates[0], near_gates[1], near_gates[2]
+    x_route, y_route = near_routes[0], near_routes[1]
+    x_gate, y_gate = near_gates[0], near_gates[1]
     coefficients(1, jnp.where(low, x_route, y_route), jnp.where(low, x_gate, y_gate))
-    norm(1)
-    expert(mine.at[1])
-    common(1)
-    lent_in(1, 0, half, 0)
-    lent_in(1, half, half, 1)
-    serve(1)
-    landed(2, half, quarter, 2)
-    landed(2, 0, quarter, 0)
-
-    arrived(theirs.at[1], result_recv.at[1])
-    merge(1)
-    for first, peer in ((0, nx), (1, ny)):
-        send(
-            at_rows(merged.at[1], first * half, half),
-            at_rows(back.at[first], first * half, half),
-            back_recv.at[first, steps],
-            peer,
-        )
-    coefficients(3, d_route, d_gate)
     coefficients(
         2,
         jnp.where(low, y_route, x_route),
         jnp.where(low, y_gate, x_gate),
         relayed=True,
     )
+
+    landed(1, 0, half, 0)
+    token_send(1, 0, quarter, 3, 4, ny)
+    token_send(1, quarter, quarter, 3, 5, ny)
+    lend(1, 0, half)
+    landed(1, half, half, 1)
+    token_send(1, half, quarter, 3, 4, nx)
+    token_send(1, half + quarter, quarter, 3, 5, nx)
+    lend(1, half, half)
+    token_send(0, half + quarter, quarter, 2, 3, nx)
+    token_send(0, quarter, quarter, 2, 3, ny)
+    arrived(at_rows(near_routes, 0, 2), meta_recv.at[1])
+    d_route = near_routes[2]
+    tally[0] = tallied(routes[...]) + tallied(x_route) + tallied(y_route) + tallied(d_route)
+    tally_send(0, 1, 4, 0, {"tp": sib})
+    norm(1)
+    expert(mine.at[1])
+    arrived(tally.at[1], tally_recv.at[0])
+    tally[2] = tally[0] + tally[1]
+    rounds = list(range(eps))
+    along_column(rounds[:1])
+    serve(1)
+    common(1)
+    coefficients(3, d_route, near_gates[2])
     arrived(theirs.at[0], result_recv.at[0])
     into_sum(base, 0)
-
-    landed(3, 0, half, 0)
-    landed(3, half, half, 1)
+    landed(2, 0, half, 2)
+    lend(2, half, quarter)
+    lend(2, 0, quarter)
+    along_column(rounds[1:2])
+    arrived(theirs.at[1], result_recv.at[1])
+    merge(1, lambda first: back.at[first], lambda step: back_recv.at[steps])
+
+    landed(3, 0, half, 4)
+    lend(3, 0, quarter)
+    lend(3, half, quarter)
+    landed(3, 0, half, 5)
+    lend(3, quarter, quarter)
+    lend(3, half + quarter, quarter)
+    along_column(rounds[2:3])
     norm(3)
     expert(mine.at[3])
+    serve(3)
     common(3)
-    lent_in(3, 0, half, 0)
-    lent_in(3, half, half, 1)
-    serve(3)
-    landed(2, half + quarter, quarter, 3)
-    landed(2, quarter, quarter, 1)
+    landed(2, 0, half, 3)
+    lend(2, half + quarter, quarter)
+    lend(2, quarter, quarter)
+    along_column(rounds[3:])
+
+    @pl.when(column_head)
+    def _():
+        tally[7] = tally[5] + tally[6] - tally[2]
+
+    hand_on(0)
     arrived(theirs.at[3], result_recv.at[3])
-    merge(3)
-    for step in range(steps):
-        for first, peer in ((0, nx), (1, ny)):
-            start = first * half + step * piece
-            send(
-                at_rows(merged.at[3], start, piece),
-                at_rows(passed, start, piece),
-                passed_recv.at[first, step],
-                peer,
-            )
+    merge(3, lambda first: passed, lambda step: passed_recv.at[step])
+    serve(2)
     norm(2)
     expert(mine.at[2])
     common(2)
-    for number in range(4):
-        lent_in(2, number * quarter, quarter, number)
-    serve(2)
-
-    expert_ids = lax.broadcasted_iota(jnp.int32, (n, rows), 0)
-
-    def counted(ref_of, amount, start):
-        def step(i, sums):
-            route = ref_of(i)
-            return (
-                sums
-                + (route[0:1] == expert_ids).astype(F32)
-                + (route[1:2] == expert_ids).astype(F32)
-            )
-
-        return lax.fori_loop(0, amount, step, start)
-
-    sums = counted(lambda i: group_routes[i], n, jnp.zeros((n, rows), F32))
-    for plane in planes:
-        arrived(every_routes.at[plane], far_recv.at[plane])
-        sums = counted(lambda i, plane=plane: every_routes[plane, i], n, sums)
-    counts = lax.dot_general(
-        jnp.ones((8, rows), F32),
-        sums,
-        (((1,), (1,)), ((), ())),
-        precision=lax.Precision.HIGHEST,
-        preferred_element_type=F32,
-    )
-    load[...] = counts[0:1, :] * (n / (rows * 2 * n * eps))
-
     arrived(theirs.at[2], result_recv.at[2])
     into_sum(shared.at[2], 2)
+    hand_on(1)
+    hand_on(2)
 
     for step in range(steps):
+        arrived(at_rows(passed, 0, 2 * piece), passed_recv.at[step])
         for first, peer in ((1, nx), (0, ny)):
             start = first * half + step * piece
             where = pl.ds(start, piece)
-            arrived(at_rows(passed, start, piece), passed_recv.at[first, step])
             merged[2, where] = (
                 shared[2, where] + column(2, 3, start, piece) * passed[where].astype(F32)
             ).astype(BF16)
-            send(
-                at_rows(merged.at[2], start, piece),
-                at_rows(back.at[1 - first], start, piece),
-                back_recv.at[1 - first, step],
-                peer,
-            )
-
-    for first in range(2):
-        arrived(at_rows(back.at[first], first * half, half), back_recv.at[first, steps])
+            link(merged.at[2], back.at[1 - first], start, piece, back_recv.at[step], peer)
+
+    arrived(at_rows(back.at[0], 0, rows), back_recv.at[steps])
 
     def early(i, carry):
         for first in range(2):
@@ -708,17 +724,35 @@
 
     lax.fori_loop(0, steps, early, 0)
 
+    hand_on(3)
+    hand_on(4)
+    counts = lax.dot_general(
+        jnp.ones((8, rows), F32),
+        tally[7],
+        (((1,), (1,)), ((), ())),
+        precision=lax.Precision.HIGHEST,
+        preferred_element_type=F32,
+    )
+    load[...] = counts[0:1, :] * (n / (rows * 2 * n * eps))
+
     for step in range(steps):
+        arrived(at_rows(back.at[0], 0, 2 * piece), back_recv.at[step])
         for first in range(2):
             start = (1 - first) * half + step * piece
             where = pl.ds(start, piece)
-            arrived(at_rows(back.at[first], start, piece), back_recv.at[first, step])
             out[where] = (
                 base[where] + column(0, 3 + first, start, piece) * back[first, where].astype(F32)
             ).astype(BF16)
 
-    for copy in pending:
-        copy.wait_send()
+    arrived(at_rows(blocks, 0, 6), sent.at[0])
+    arrived(blocks, sent.at[1])
+    arrived(at_rows(near_routes, 0, 2), sent.at[3])
+    arrived(tally.at[0], sent.at[4])
+    for number, test in ((5, above), (6, below), *((i, hand[i][0]) for i in hand)):
+
+        @pl.when(test)
+        def _():
+            arrived(tally.at[0], sent.at[number])
 
 
 def write_out(mixed, load, mixed_out, load_out, sem):
@@ -752,30 +786,20 @@
     vmem = pl.BlockSpec(memory_space=pltpu.VMEM)
     hbm = pl.BlockSpec(memory_space=pl.ANY)
     dma = pltpu.SemaphoreType.DMA
-    weights = [
-        pltpu.VMEM(expert_gate.shape[1:], BF16),
-        pltpu.VMEM(expert_up.shape[1:], BF16),
-        pltpu.VMEM(expert_down.shape[1:], BF16),
-        pltpu.VMEM(shared_gate.shape, BF16),
-        pltpu.VMEM(shared_up.shape, BF16),
-        pltpu.VMEM(shared_down.shape, BF16),
-        dma((6,)),
-        dma((2,)),
-        dma((n - 1,)),
-        dma((n,)),
-        dma((max(1, eps - 1),)),
-        dma((eps,)),
-    ]
     if n == 8:
         body = functools.partial(square, eps)
+        small = hbm
         scratch = [
             pltpu.VMEM((8, rows, width), BF16),
-            pltpu.VMEM((n, top, rows), jnp.int32),
-            pltpu.VMEM((eps, n, top, rows), jnp.int32),
+            pltpu.VMEM((top, rows), jnp.int32),
+            pltpu.VMEM((top, rows), F32),
+            pltpu.VMEM((1, width), F32),
+            pltpu.VMEM((3, top, rows), jnp.int32),
             pltpu.VMEM((3, top, rows), F32),
+            pltpu.VMEM((8, n, rows), F32),
             pltpu.VMEM((4, 8, rows), F32),
             pltpu.VMEM((4, rows, 8), F32),
-            pltpu.VMEM((rows, width), BF16),
+            pltpu.VMEM((2, rows, width), BF16),
             pltpu.VMEM((rows, units), BF16),
             pltpu.VMEM((4, rows, width), BF16),
             pltpu.VMEM((4, rows, width), BF16),
@@ -785,17 +809,23 @@
             pltpu.VMEM((rows, width), BF16),
             pltpu.VMEM((2, rows, width), BF16),
             pltpu.VMEM((rows, width), F32),
-            *weights,
-            dma((3,)),
-            dma((26 + rows // 8,)),
-            dma((4, 4)),
-            dma((4, 4)),
+            pltpu.VMEM((2, *expert_gate.shape[1:]), BF16),
+            pltpu.VMEM(expert_down.shape[1:], BF16),
+            pltpu.VMEM((2, *shared_gate.shape), BF16),
+            pltpu.VMEM(shared_down.shape, BF16),
+            dma((8,)),
+            dma((10,)),
+            dma((2,)),
             dma((4,)),
-            dma((2, rows // 32)),
-            dma((2, rows // 32 + 1)),
+            dma((6,)),
+            dma((4,)),
+            dma((4,)),
+            dma((rows // 32,)),
+            dma((rows // 32 + 1,)),
         ]
     else:
         body = functools.partial(direct, n, eps, cap)
+        small = vmem
         scratch = [
             pltpu.VMEM((rows, width), BF16),
             pltpu.VMEM((n, rows, width), BF16),
@@ -806,7 +836,18 @@
             pltpu.VMEM((n, cap, width), BF16),
             pltpu.VMEM((n, cap, width), BF16),
             pltpu.VMEM((rows, width), F32),
-            *weights,
+            pltpu.VMEM(expert_gate.shape[1:], BF16),
+            pltpu.VMEM(expert_up.shape[1:], BF16),
+            pltpu.VMEM(expert_down.shape[1:], BF16),
+            pltpu.VMEM(shared_gate.shape, BF16),
+            pltpu.VMEM(shared_up.shape, BF16),
+            pltpu.VMEM(shared_down.shape, BF16),
+            dma((6,)),
+            dma((2,)),
+            dma((n - 1,)),
+            dma((n,)),
+            dma((max(1, eps - 1),)),
+            dma((eps,)),
             dma((2 * (n - 1),)),
             dma((n, 2)),
             dma((n,)),
@@ -818,7 +859,7 @@
             pltpu.VMEM((rows, width), BF16),
             pltpu.VMEM((1, n), F32),
         ),
-        in_specs=[hbm] + [vmem] * 3 + [hbm] * 6,
+        in_specs=[hbm] + [small] * 3 + [hbm] * 6,
         out_specs=(vmem, vmem),
         scratch_shapes=scratch,
         compiler_params=pltpu.CompilerParams(

time: 45.8 us -> 41 us (0.90)
  Pallas kernels: 44.7 us -> 40.1 us
    pallas_call x1, Pallas kernels: 43.9 us -> 39.2 us  [per_device(): pl.pallas_call(body, out_shape=(pltpu.VMEM((rows, width), BF16), pltpu.VM...]
where the time goes in v2:
time: 41 us; the launch traced here: 40.9 us
  Pallas kernels  40.1 us (98%)
  between operations  0.8 us (2%)
    pallas_call x1, Pallas kernels, per_device(): pl.pallas_call(body, out_shape=(pltpu.VMEM((rows, width), BF16), pltpu.VM...  39.2 us

profile of v2, /device:TPU:0, one launch (start us, length us, event | category | flops | bytes accessed | tf_op | source)
XLA Modules:
  0.0 40.9 jit_solution(18031096994299726818)
XLA Ops:
  0.6 39.2 %shard_map.113 = (bf16[128,2048]{1,0:T(8,128)(2,1)S(1)}, f32[1,8]{1,0:T(1,128)S(1)}) custom-call(bf16[128,2048]{1,0:T(8,128)(2,1)} %tokens_hbm.1, s32[2,128]{1,0:T(2,128)} %bitcast.5, f32[2,128]{1,0:T(2,128)} %bitcast.6, f32[1,2048]{1,0:T(1,128)} %bitcast.4, bf16[1,2048,512]{2,1,0:T(8,128)(2,1)} %expert_gate.1, bf16[1,2048,512]{2,1,0:T(8,128)(2,1)} %expert_up.1, ...), custom_call_target="tpu_custom_call" | custom-call | tf_op jit(solution)/shard_map/pallas_call | solution.py:856
  39.9 0.8 %shard_map.114 = (bf16[128,2048]{1,0:T(8,128)(2,1)}, f32[1,8]{1,0:T(1,128)}) custom-call(bf16[128,2048]{1,0:T(8,128)(2,1)S(1)} %get-tuple-element.6.mixed, f32[1,8]{1,0:T(1,128)S(1)} %get-tuple-element.7.load), custom_call_target="tpu_custom_call" | custom-call | tf_op jit(solution)/shard_map/pallas_call | solution.py:880

commit v3 on v2

--- a/solution.py
+++ b/solution.py
@@ -325,8 +325,8 @@
     w_down,
     s_in,
     s_down,
-    own_sem,
-    sent,
+    sems,
+    entered,
     meta_recv,
     tally_recv,
     token_recv,
@@ -351,22 +351,11 @@
     column_head = me == 0
     below, above = column_head & (here > 0), column_head & (here < eps - 1)
 
-    barrier = pltpu.get_barrier_semaphore()
-    for peer in (sib, nx, ny):
-        pl.semaphore_signal(barrier, inc=1, device_id={"tp": peer})
-
-    @pl.when(below)
-    def _():
-        pl.semaphore_signal(barrier, inc=1, device_id={"ep": here - 1})
-
-    @pl.when(above)
-    def _():
-        pl.semaphore_signal(barrier, inc=1, device_id={"ep": here + 1})
-
     copies = [
-        (0, tokens_hbm, blocks.at[0]),
-        (1, routes_hbm, routes),
+        (2, routes_hbm, routes),
         (2, gates_hbm, gates),
+        (0, tokens_hbm.at[pl.ds(0, half)], blocks.at[0, pl.ds(0, half)]),
+        (1, tokens_hbm.at[pl.ds(half, half)], blocks.at[0, pl.ds(half, half)]),
         (3, gain_hbm, gain),
         (4, expert_gate.at[0], w_in.at[0]),
         (4, expert_up.at[0], w_in.at[1]),
@@ -375,13 +364,41 @@
         (6, shared_up, s_in.at[1]),
         (7, shared_down, s_down),
     ]
-    for number, source, target in copies:
-        pltpu.make_async_copy(source, target, own_sem.at[number]).start()
+    for number, source, target in copies[:4]:
+        pltpu.make_async_copy(source, target, sems.at[number]).start()
+
+    barrier = pltpu.get_barrier_semaphore()
+    edges = [(core, sib), (xbit, nx), (ybit, ny)]
+    for bit, peer in edges:
+
+        @pl.when(bit == 0)
+        def _():
+            pl.semaphore_signal(barrier, inc=1, device_id={"tp": peer})
+
+    @pl.when(above)
+    def _():
+        pl.semaphore_signal(barrier, inc=1, device_id={"ep": here + 1})
+
+    for number, source, target in copies[4:]:
+        pltpu.make_async_copy(source, target, sems.at[number]).start()
 
     def arrived(ref, sem):
         pltpu.make_async_copy(ref, ref, sem).wait()
 
-    pl.semaphore_wait(barrier, 3 + jnp.where(below, 1, 0) + jnp.where(above, 1, 0))
+
+    @pl.when(me + here > 0)
+    def _():
+        pl.semaphore_wait(barrier, core + xbit + ybit + jnp.where(below, 1, 0))
+
+    for number, (bit, peer) in enumerate(edges):
+
+        @pl.when(bit == 1)
+        def _():
+            pl.semaphore_signal(entered.at[number], inc=1, device_id={"tp": peer})
+
+    @pl.when(below)
+    def _():
+        pl.semaphore_signal(entered.at[3], inc=1, device_id={"ep": here - 1})
 
     def send(source, target, send_sem, recv_sem, where):
         pltpu.make_async_remote_copy(
@@ -399,7 +416,7 @@
         send(
             at_rows(source, start, size),
             at_rows(target, start, size),
-            sent.at[0],
+            sems.at[0],
             recv_sem,
             {"tp": peer},
         )
@@ -411,7 +428,7 @@
         send(
             at_rows(blocks.at[group], start, size),
             at_rows(blocks.at[group + 4], start, size),
-            sent.at[1],
+            sems.at[1],
             core_recv.at[group],
             {"tp": sib},
         )
@@ -419,15 +436,40 @@
     def landed(group, start, size, number):
         arrived(at_rows(blocks.at[group], start, size), token_recv.at[number])
 
-    arrived(routes, own_sem.at[1])
-    arrived(gates, own_sem.at[2])
-    for i, peer in enumerate((nx, ny)):
-        send(routes, near_routes.at[i], sent.at[2], meta_recv.at[0], {"tp": peer})
-        send(gates, near_gates.at[i], sent.at[2], meta_recv.at[0], {"tp": peer})
-    arrived(blocks.at[0], own_sem.at[0])
-    token_send(0, 0, half, 1, 0, nx)
-    token_send(0, half, half, 1, 1, ny)
+    def introduce(i):
+        peer = (nx, ny)[i]
+        send(routes, near_routes.at[i], sems.at[2], meta_recv.at[0], {"tp": peer})
+        send(gates, near_gates.at[i], sems.at[2], meta_recv.at[0], {"tp": peer})
+
+    def open_link(i):
+        token_send(0, i * half, half, 1, i, (nx, ny)[i])
+
+    arrived(at_rows(near_routes, 0, 2), sems.at[2])
+    for i in range(2):
+
+        @pl.when(edges[1 + i][0] == 1)
+        def _():
+            introduce(i)
+
+    for i in range(2):
+        arrived(blocks.at[0, pl.ds(i * half, half)], sems.at[i])
+
+        @pl.when(edges[1 + i][0] == 1)
+        def _():
+            open_link(i)
+
+    @pl.when(core == 0)
+    def _():
+        pl.semaphore_wait(entered.at[0], 1)
+
     lend(0, 0, rows)
+    for i in range(2):
+
+        @pl.when(edges[1 + i][0] == 0)
+        def _():
+            pl.semaphore_wait(entered.at[1 + i], 1)
+            introduce(i)
+            open_link(i)
 
     expert_ids = lax.broadcasted_iota(jnp.int32, (n, rows), 0)
 
@@ -435,7 +477,7 @@
         return (route[0:1] == expert_ids).astype(F32) + (route[1:2] == expert_ids).astype(F32)
 
     def tally_send(source, target, number, recv, where):
-        send(tally.at[source], tally.at[target], sent.at[number], tally_recv.at[recv], where)
+        send(tally.at[source], tally.at[target], sems.at[number], tally_recv.at[recv], where)
 
     def along_column(rounds):
         for r in rounds:
@@ -448,7 +490,7 @@
                     value = value + tally[3]
                 tally[5] = value
                 if r < eps - 1:
-                    tally_send(5, 3, 5, 1, {"ep": here + 1})
+                    tally_send(5, 3, 3, 1, {"ep": here + 1})
 
             @pl.when(column_head & (here == eps - 1 - r))
             def _():
@@ -458,30 +500,25 @@
                     value = value + tally[4]
                 tally[6] = value
                 if r < eps - 1:
-                    tally_send(6, 4, 6, 2, {"ep": here - 1})
-
-    hand = {
-        7: (core == 0, sib),
-        8: (column_head, nx),
-        9: ((core == 0) & (ybit == 0), ny),
-    }
+                    tally_send(6, 4, 4, 2, {"ep": here - 1})
+
     handers = [
-        (column_head, (7, 8, 9)),
-        ((core == 0) & (xbit == 1) & (ybit == 0), (7, 9)),
-        ((core == 0) & (xbit == 0) & (ybit == 1), (7,)),
-        ((core == 0) & (xbit == 1) & (ybit == 1), (7,)),
+        (column_head, (sib, nx, ny)),
+        ((core == 0) & (xbit == 1) & (ybit == 0), (sib, ny)),
+        ((core == 0) & (xbit == 0) & (ybit == 1), (sib,)),
+        ((core == 0) & (xbit == 1) & (ybit == 1), (sib,)),
         (core == 1, ()),
     ]
 
     def hand_on(number):
-        test, numbers = handers[number]
+        test, peers = handers[number]
 
         @pl.when(test)
         def _():
             if number > 0:
                 arrived(tally.at[7], tally_recv.at[3])
-            for i in numbers:
-                tally_send(7, 7, i, 3, {"tp": hand[i][1]})
+            for peer in peers:
+                tally_send(7, 7, 2, 3, {"tp": peer})
 
     def norm(group, slot=0):
         values = blocks[group].astype(F32)
@@ -515,7 +552,7 @@
         arrived(blocks.at[group + 4], core_recv.at[group])
         norm(group + 4, 1)
         expert(lent.at[group], 1)
-        send(lent.at[group], theirs.at[group], sent.at[1], result_recv.at[group], {"tp": sib})
+        send(lent.at[group], theirs.at[group], sems.at[1], result_recv.at[group], {"tp": sib})
 
     def named(ids):
         def test(route):
@@ -610,20 +647,20 @@
                 merged[group, pl.ds(start, piece)] = local_sum(group, start, piece).astype(BF16)
                 link(merged.at[group], target_of(first), start, piece, recv_of(step), peer)
 
-    arrived(gain, own_sem.at[3])
+    arrived(gain, sems.at[3])
     norm(0)
-    arrived(w_in, own_sem.at[4])
-    arrived(w_down, own_sem.at[5])
+    arrived(w_in, sems.at[4])
+    arrived(w_down, sems.at[5])
     expert(mine.at[0])
-    arrived(s_in, own_sem.at[6])
-    arrived(s_down, own_sem.at[7])
+    arrived(s_in, sems.at[6])
+    arrived(s_down, sems.at[7])
     common(0)
     serve(0)
 
     arrived(tally.at[0], meta_recv.at[0])
-    arrived(tally.at[0], sent.at[2])
-    send(near_routes.at[0], near_routes.at[2], sent.at[3], meta_recv.at[1], {"tp": ny})
-    send(near_gates.at[0], near_gates.at[2], sent.at[3], meta_recv.at[1], {"tp": ny})
+    arrived(tally.at[0], sems.at[2])
+    send(near_routes.at[0], near_routes.at[2], sems.at[2], meta_recv.at[1], {"tp": ny})
+    send(near_gates.at[0], near_gates.at[2], sems.at[2], meta_recv.at[1], {"tp": ny})
     token_send(0, half, quarter, 2, 2, nx)
     token_send(0, 0, quarter, 2, 2, ny)
     own_coefficients()
@@ -650,12 +687,19 @@
     arrived(at_rows(near_routes, 0, 2), meta_recv.at[1])
     d_route = near_routes[2]
     tally[0] = tallied(routes[...]) + tallied(x_route) + tallied(y_route) + tallied(d_route)
-    tally_send(0, 1, 4, 0, {"tp": sib})
+    arrived(at_rows(near_routes, 0, 2), sems.at[2])
+    tally_send(0, 1, 2, 0, {"tp": sib})
     norm(1)
     expert(mine.at[1])
     arrived(tally.at[1], tally_recv.at[0])
+    arrived(tally.at[0], sems.at[2])
     tally[2] = tally[0] + tally[1]
     rounds = list(range(eps))
+
+    @pl.when(above)
+    def _():
+        pl.semaphore_wait(entered.at[3], 1)
+
     along_column(rounds[:1])
     serve(1)
     common(1)
@@ -677,9 +721,9 @@
     lend(3, half + quarter, quarter)
     along_column(rounds[2:3])
     norm(3)
+    common(3)
+    serve(3)
     expert(mine.at[3])
-    serve(3)
-    common(3)
     landed(2, 0, half, 3)
     lend(2, half + quarter, quarter)
     lend(2, quarter, quarter)
@@ -744,15 +788,19 @@
                 base[where] + column(0, 3 + first, start, piece) * back[first, where].astype(F32)
             ).astype(BF16)
 
-    arrived(at_rows(blocks, 0, 6), sent.at[0])
-    arrived(blocks, sent.at[1])
-    arrived(at_rows(near_routes, 0, 2), sent.at[3])
-    arrived(tally.at[0], sent.at[4])
-    for number, test in ((5, above), (6, below), *((i, hand[i][0]) for i in hand)):
+    arrived(at_rows(blocks, 0, 6), sems.at[0])
+    arrived(blocks, sems.at[1])
+    for number, test in ((3, above), (4, below)):
 
         @pl.when(test)
         def _():
-            arrived(tally.at[0], sent.at[number])
+            arrived(tally.at[0], sems.at[number])
+
+    for test, peers in handers[:-1]:
+
+        @pl.when(test)
+        def _():
+            arrived(at_rows(tally, 0, len(peers)), sems.at[2])
 
 
 def write_out(mixed, load, mixed_out, load_out, sem):
@@ -786,7 +834,7 @@
     vmem = pl.BlockSpec(memory_space=pltpu.VMEM)
     hbm = pl.BlockSpec(memory_space=pl.ANY)
     dma = pltpu.SemaphoreType.DMA
-    if n == 8:
+    if n == 8 and top == 2:
         body = functools.partial(square, eps)
         small = hbm
         scratch = [
@@ -814,7 +862,7 @@
             pltpu.VMEM((2, *shared_gate.shape), BF16),
             pltpu.VMEM(shared_down.shape, BF16),
             dma((8,)),
-            dma((10,)),
+            pltpu.SemaphoreType.REGULAR((4,)),
             dma((2,)),
             dma((4,)),
             dma((6,)),

time: 41 us -> 40.8 us (level)
  no operation moved by 1% of the time
where the time goes in v3:
time: 40.8 us; the launch traced here: 40.6 us
  Pallas kernels  39.8 us (98%)
  between operations  0.8 us (2%)
    pallas_call x1, Pallas kernels, per_device(): pl.pallas_call(body, out_shape=(pltpu.VMEM((rows, width), BF16), pltpu.VM...  39 us

profile of v3, /device:TPU:0, one launch (start us, length us, event | category | flops | bytes accessed | tf_op | source)
XLA Modules:
  0.0 40.6 jit_solution(11475246960239772345)
XLA Ops:
  0.6 39.0 %shard_map.113 = (bf16[128,2048]{1,0:T(8,128)(2,1)S(1)}, f32[1,8]{1,0:T(1,128)S(1)}) custom-call(bf16[128,2048]{1,0:T(8,128)(2,1)} %tokens_hbm.1, s32[2,128]{1,0:T(2,128)} %bitcast.5, f32[2,128]{1,0:T(2,128)} %bitcast.6, f32[1,2048]{1,0:T(1,128)} %bitcast.4, bf16[1,2048,512]{2,1,0:T(8,128)(2,1)} %expert_gate.1, bf16[1,2048,512]{2,1,0:T(8,128)(2,1)} %expert_up.1, ...), custom_call_target="tpu_custom_call" | custom-call | tf_op jit(solution)/shard_map/pallas_call | solution.py:904
  39.6 0.8 %shard_map.114 = (bf16[128,2048]{1,0:T(8,128)(2,1)}, f32[1,8]{1,0:T(1,128)}) custom-call(bf16[128,2048]{1,0:T(8,128)(2,1)S(1)} %get-tuple-element.6.mixed, f32[1,8]{1,0:T(1,128)S(1)} %get-tuple-element.7.load), custom_call_target="tpu_custom_call" | custom-call | tf_op jit(solution)/shard_map/pallas_call | solution.py:928

commit v4 on v3

--- a/solution.py
+++ b/solution.py
@@ -429,7 +429,7 @@
             at_rows(blocks.at[group], start, size),
             at_rows(blocks.at[group + 4], start, size),
             sems.at[1],
-            core_recv.at[group],
+            core_recv.at[group % 2],
             {"tp": sib},
         )
 
@@ -549,10 +549,10 @@
             )
 
     def serve(group):
-        arrived(blocks.at[group + 4], core_recv.at[group])
+        arrived(blocks.at[group + 4], core_recv.at[group % 2])
         norm(group + 4, 1)
         expert(lent.at[group], 1)
-        send(lent.at[group], theirs.at[group], sems.at[1], result_recv.at[group], {"tp": sib})
+        send(lent.at[group], theirs.at[group], sems.at[1], result_recv.at[group % 2], {"tp": sib})
 
     def named(ids):
         def test(route):
@@ -734,13 +734,13 @@
         tally[7] = tally[5] + tally[6] - tally[2]
 
     hand_on(0)
-    arrived(theirs.at[3], result_recv.at[3])
+    arrived(theirs.at[3], result_recv.at[1])
     merge(3, lambda first: passed, lambda step: passed_recv.at[step])
     serve(2)
     norm(2)
     expert(mine.at[2])
     common(2)
-    arrived(theirs.at[2], result_recv.at[2])
+    arrived(theirs.at[2], result_recv.at[0])
     into_sum(shared.at[2], 2)
     hand_on(1)
     hand_on(2)
@@ -866,8 +866,8 @@
             dma((2,)),
             dma((4,)),
             dma((6,)),
-            dma((4,)),
-            dma((4,)),
+            dma((2,)),
+            dma((2,)),
             dma((rows // 32,)),
             dma((rows // 32 + 1,)),
         ]

time: 40.8 us -> 40.7 us (level)
  no operation moved by 1% of the time
where the time goes in v4:
time: 40.7 us; the launch traced here: 40.6 us
  Pallas kernels  39.8 us (98%)
  between operations  0.8 us (2%)
    pallas_call x1, Pallas kernels, per_device(): pl.pallas_call(body, out_shape=(pltpu.VMEM((rows, width), BF16), pltpu.VM...  38.9 us
    pallas_call x1, Pallas kernels, per_device(): pl.pallas_call(write_out, out_shape=(jax.ShapeDtypeStruct((rows, width),...  0.81 us

profile of v4, /device:TPU:0, one launch (start us, length us, event | category | flops | bytes accessed | tf_op | source)
XLA Modules:
  0.0 40.6 jit_solution(16337759805943614817)
XLA Ops:
  0.6 38.9 %shard_map.113 = (bf16[128,2048]{1,0:T(8,128)(2,1)S(1)}, f32[1,8]{1,0:T(1,128)S(1)}) custom-call(bf16[128,2048]{1,0:T(8,128)(2,1)} %tokens_hbm.1, s32[2,128]{1,0:T(2,128)} %bitcast.5, f32[2,128]{1,0:T(2,128)} %bitcast.6, f32[1,2048]{1,0:T(1,128)} %bitcast.4, bf16[1,2048,512]{2,1,0:T(8,128)(2,1)} %expert_gate.1, bf16[1,2048,512]{2,1,0:T(8,128)(2,1)} %expert_up.1, ...), custom_call_target="tpu_custom_call" | custom-call | tf_op jit(solution)/shard_map/pallas_call | solution.py:904
  39.6 0.8 %shard_map.114 = (bf16[128,2048]{1,0:T(8,128)(2,1)}, f32[1,8]{1,0:T(1,128)}) custom-call(bf16[128,2048]{1,0:T(8,128)(2,1)S(1)} %get-tuple-element.6.mixed, f32[1,8]{1,0:T(1,128)S(1)} %get-tuple-element.7.load), custom_call_target="tpu_custom_call" | custom-call | tf_op jit(solution)/shard_map/pallas_call | solution.py:928
